TPU v7x, 256 devices: a whole 4x4x8 slice. The times are simulated.
256 devices in a mesh: ep: 64 (over z, x, core), tp: 4 (over y).
Axes of the slice: x: 4, y: 4, z: 8, core: 2. Of those that a mesh axis runs over, the one named last changes fastest.
Arguments:
- projected_queries: bfloat16 [16384, 2048], P('ep', 'tp'), may hold values from -245 to 245, as said below
- key_proj: bfloat16 [16384, 512], P('ep', 'tp'), may hold values from -6.2 to 6.2
- projected_values: bfloat16 [16384, 512], P('ep', 'tp'), may hold values from -24 to 24
- head_sink_logits: float32 [32], P('tp'), may hold values from 1 to 6
- out_weight: bfloat16 [2048, 4096], P('tp'), may hold values from -0.125 to 0.125
- expert_input: bfloat16 [8192, 4096], P('ep'), may hold values from -6 to 6
- norm_gain: float32 [4096], replicated, may hold values from 0.1 to 1.9
- routing: int32 [8192, 4], P('ep'), may hold values from 0 to 63, all different within a row; in each aligned block of 128 rows (0 to 127, 128 to 255, ...) at most 12 rows name the same one
- route_weight: float32 [8192, 4], P('ep'), may hold values from 0.1 to 1
- gate_weight: bfloat16 [64, 4096, 1024], P('ep', None, 'tp'), may hold values from -0.27929688 to 0.27929688
- up_weight: bfloat16 [64, 4096, 1024], P('ep', None, 'tp'), may hold values from -0.27929688 to 0.27929688
- down_weight: bfloat16 [64, 1024, 4096], P('ep', 'tp'), may hold values from -0.046875 to 0.046875
Outputs:
- mixer_output: bfloat16 [16384, 4096], P(('ep', 'tp'))
- expert_output: bfloat16 [8192, 4096], P('ep', 'tp')
Inputs may be any that keep to these rules, and one draw needn't show every extreme that they name: `projected_queries`: in the hidden draw some queries nearly equal a large multiple of a nearby key. `routing`: each row names 4 different experts; among the rows of one device (aligned blocks of 128 rows) no expert is named more than 12 times, a bound that some block reaches.
All inputs are finite; a program needn't handle non-finite values.
Results may differ from a plain program's by a relative error of at most 0.014.
Values may be sent and summed in bfloat16 or wider, within the bound.
A program may use at most 128 MiB of HBM per device.

v0:
```python
import jax
import jax.numpy as jnp
from jax import lax
from jax.sharding import PartitionSpec as P

D = 4096
HEAD_SIZE = 64
WINDOW_KEYS = 128
TOPK = 4
EPS = 1e-06
CLAMP = 7.0
SLOPE = 1.702


def passed_along(block, axis, distance):
    devices = range(lax.axis_size(axis))
    route = [(i - distance, i) for i in devices if i - distance in devices]
    return lax.ppermute(block, axis, route)


def shards(
    projected_queries,
    key_proj,
    projected_values,
    head_sink_logits,
    out_weight,
    expert_input,
    norm_gain,
    routing,
    route_weight,
    gate_weight,
    up_weight,
    down_weight,
):
    query_rows = projected_queries.shape[0]
    kv_heads = key_proj.shape[1] // HEAD_SIZE
    heads_per_group = projected_queries.shape[1] // HEAD_SIZE // kv_heads
    count_of_blocks = query_rows // WINDOW_KEYS
    prior_key, prior_value = passed_along(
        (key_proj[query_rows - WINDOW_KEYS :], projected_values[query_rows - WINDOW_KEYS :]),
        "ep",
        1,
    )
    key_all = jnp.concatenate([prior_key, key_proj], axis=0)
    value_all = jnp.concatenate([prior_value, projected_values], axis=0)
    window_keys = jnp.concatenate(
        [
            key_all[:-WINDOW_KEYS].reshape(count_of_blocks, WINDOW_KEYS, kv_heads, HEAD_SIZE),
            key_all[WINDOW_KEYS:].reshape(count_of_blocks, WINDOW_KEYS, kv_heads, HEAD_SIZE),
        ],
        axis=1,
    )
    window_values = jnp.concatenate(
        [
            value_all[:-WINDOW_KEYS].reshape(count_of_blocks, WINDOW_KEYS, kv_heads, HEAD_SIZE),
            value_all[WINDOW_KEYS:].reshape(count_of_blocks, WINDOW_KEYS, kv_heads, HEAD_SIZE),
        ],
        axis=1,
    )
    query_blocks = projected_queries.reshape(
        count_of_blocks, WINDOW_KEYS, kv_heads, heads_per_group, HEAD_SIZE
    )
    scores = jnp.einsum(
        "nqhgd,nshd->nhgqs", query_blocks, window_keys, preferred_element_type=jnp.float32
    ) * HEAD_SIZE ** (-0.5)
    offset = lax.axis_index("ep") * query_rows
    block_ids = jnp.arange(count_of_blocks)[:, None, None] * WINDOW_KEYS + offset
    query_pos = block_ids + jnp.arange(WINDOW_KEYS)[None, :, None]
    key_pos = block_ids - WINDOW_KEYS + jnp.arange(2 * WINDOW_KEYS)[None, None, :]
    permitted_mask = (key_pos <= query_pos) & (query_pos - key_pos < WINDOW_KEYS) & (key_pos >= 0)
    scores = jnp.where(permitted_mask[:, None, None, :, :], scores, -jnp.inf)
    sink_col = head_sink_logits.reshape(kv_heads, heads_per_group)[None, :, :, None, None]
    highest = jnp.maximum(jnp.max(scores, axis=-1, keepdims=True), sink_col)
    numerator = jnp.exp(scores - highest)
    denominator = jnp.sum(numerator, axis=-1, keepdims=True) + jnp.exp(sink_col - highest)
    weights = (numerator / denominator).astype(jnp.bfloat16)
    attended = jnp.einsum(
        "nhgqs,nshd->nqhgd", weights, window_values, preferred_element_type=jnp.float32
    )
    attended = attended.astype(jnp.bfloat16).reshape(
        query_rows, kv_heads * heads_per_group * HEAD_SIZE
    )
    mixer_output = lax.psum_scatter(
        jnp.dot(attended, out_weight, preferred_element_type=jnp.float32).astype(jnp.bfloat16),
        "tp",
        scatter_dimension=0,
        tiled=True,
    )
    token_rows = expert_input.shape[0]
    experts = lax.axis_size("ep")
    capacity = max(3 * token_rows * TOPK // (2 * experts), 2)
    col_share = D // lax.axis_size("tp")
    widened = expert_input.astype(jnp.float32)
    normed = (
        widened
        * lax.rsqrt(jnp.mean(widened * widened, axis=-1, keepdims=True) + EPS)
        * norm_gain[None, :]
    ).astype(jnp.bfloat16)
    flat_ids = routing.reshape(-1)
    onehot = (flat_ids[:, None] == jnp.arange(experts, dtype=jnp.int32)[None, :]).astype(jnp.int32)
    rank_in = jnp.cumsum(onehot, axis=0) - 1
    target = flat_ids * capacity + jnp.sum(rank_in * onehot, axis=1)
    tok_ids = jnp.arange(token_rows * TOPK) // TOPK
    slot_tok = jnp.full((experts * capacity,), token_rows, jnp.int32).at[target].set(tok_ids)
    gate_one = gate_weight[0]
    up_one = up_weight[0]
    own_cols = lax.dynamic_slice_in_dim(normed, lax.axis_index("tp") * col_share, col_share, 1)
    extended = jnp.concatenate([own_cols, jnp.zeros((1, col_share), jnp.bfloat16)], axis=0)
    outgoing = jnp.take(extended, slot_tok, axis=0).reshape(experts, capacity, col_share)
    arrived = lax.all_to_all(outgoing, "ep", split_axis=0, concat_axis=0, tiled=True).reshape(
        experts * capacity, col_share
    )
    portion = lax.all_gather(arrived, "tp", axis=1, tiled=True)
    gate_pre = jnp.dot(portion, gate_one, preferred_element_type=jnp.float32)
    up_pre = jnp.dot(portion, up_one, preferred_element_type=jnp.float32)
    gate_cut = jnp.minimum(gate_pre, CLAMP)
    activated = (
        (jnp.clip(up_pre, -CLAMP, CLAMP) + 1.0) * gate_cut * jax.nn.sigmoid(SLOPE * gate_cut)
    ).astype(jnp.bfloat16)
    down_cols = lax.all_to_all(down_weight[0], "tp", split_axis=1, concat_axis=0, tiled=True)
    expert_result = jnp.dot(
        lax.all_gather(activated, "tp", axis=1, tiled=True),
        down_cols,
        preferred_element_type=jnp.float32,
    ).astype(jnp.bfloat16)
    returned = lax.all_to_all(
        expert_result.reshape(experts, capacity, col_share),
        "ep",
        split_axis=0,
        concat_axis=0,
        tiled=True,
    )
    picked = jnp.take(returned.reshape(experts * capacity, col_share), target, axis=0)
    picked = picked.astype(jnp.float32).reshape(token_rows, TOPK, col_share)
    expert_output = jnp.sum(picked * route_weight[:, :, None], axis=1).astype(jnp.bfloat16)
    return (mixer_output, expert_output)


def solution(mesh):
    placed = (
        P("ep", "tp"),
        P("ep", "tp"),
        P("ep", "tp"),
        P("tp"),
        P("tp", None),
        P("ep", None),
        P(),
        P("ep", None),
        P("ep", None),
        P("ep", None, "tp"),
        P("ep", None, "tp"),
        P("ep", "tp", None),
    )
    return jax.shard_map(
        shards,
        mesh=mesh,
        in_specs=placed,
        out_specs=(P(("ep", "tp"), None), P("ep", "tp")),
        check_vma=False,
    )
```

profile of v0, /device:TPU:2, one launch (start us, length us, event | category | flops | bytes accessed | tf_op | source)
XLA Modules:
  0.0 303.8 jit_solution(12836123487075077681)
XLA Ops:
  7.2 2.9 convert_element_type.41
  12.7 2.4 scatter_custom_fusion
  17.1 3.6 %gather_fusion = bf16[768,1024]{1,0:T(8,128)(2,1)} fusion(bf16[129,1024]{1,0:T(8,128)(2,1)S(1)} %concatenate.19, s32[1024]{0:T(1024)S(1)} %pad_clamp_fusion.1), kind=kCustom, calls=%fused_computation | custom fusion | bytes 3148800 | tf_op jit(solution)/shard_map/jit(_take)/gather | solution.py:109
  20.6 3.6 %gather.13 = bf16[64,12,1024]{2,1,0:T(8,128)(2,1)} reshape(bf16[768,1024]{1,0:T(8,128)(2,1)} %gather_fusion) | data formatting | bytes 3145728 | tf_op jit(solution)/shard_map/jit(_take)/gather | solution.py:109
  26.2 63.2 %all_to_all.29 = bf16[64,12,1024]{2,1,0:T(8,128)(2,1)} all-to-all(bf16[64,12,1024]{2,1,0:T(8,128)(2,1)S(1)} %broadcast_select_fusion), channel_id=1, replica_groups=mesh['ep'=64,'tp'=4] {'ep'}, dimensions={0} | all-to-all | bytes 3145728 | tf_op jit(solution)/shard_map/all_to_all | solution.py:110
  89.4 3.6 %reshape.225 = bf16[768,1024]{1,0:T(8,128)(2,1)} reshape(bf16[64,12,1024]{2,1,0:T(8,128)(2,1)} %all_to_all.29) | data formatting | bytes 3145728 | tf_op jit(solution)/shard_map/reshape | solution.py:110
  93.0 4.1 %copy.72 = bf16[1,256,4096]{1,2,0:T(8,128)(2,1)} copy(bf16[1,256,4096]{2,1,0:T(8,128)(2,1)} %param.23) | data formatting | bytes 4194304 | tf_op args[11]
  97.1 4.6 %all-to-all-start.1 = ((bf16[256,4,1024]{0,2,1:T(8,128)(2,1)}), bf16[256,4,1024]{0,2,1:T(8,128)(2,1)}, u32[]{:S(2)}, u32[]{:S(2)}) async-start(bf16[256,4,1024]{0,2,1:T(8,128)(2,1)} %bitcast.66), calls=%async_computation.2 | async-start | bytes 4194304 | tf_op jit(solution)/shard_map/all_to_all | solution.py:120
  101.8 1.9 collective-permute-start.1
  103.7 3.5 %collective-permute-start = (bf16[128,128]{1,0:T(8,128)(2,1)S(1)}, bf16[128,128]{1,0:T(8,128)(2,1)S(1)}, u32[]{:S(2)}, u32[]{:S(2)}) collective-permute-start(bf16[128,128]{1,0:T(8,128)(2,1)S(1)} %slice.18), channel_id=1, source_target_pairs={{0,4},{4,8},{8,12},{12,16},{16,20},{20,24},{24,28},{28,32},{32,36}... | collective-permute-start | bytes 98312 | tf_op jit(solution)/shard_map/ppermute | solution.py:18
  107.4 70.1 %all-gather.3.cloned.1.call-done = bf16[768,4096]{1,0:T(8,128)(2,1)} async-done(((bf16[768,1024]{1,0:T(8,128)(2,1)}), bf16[768,4096]{1,0:T(8,128)(2,1)}) %all-gather.3.cloned.1.call-update) | async-done | bytes 6291472 | tf_op jit(solution)/shard_map/all_gather | solution.py:113
  177.5 4.7 %fusion.8 = f32[768,256]{1,0:T(8,128)S(1)} fusion(bf16[768,4096]{1,0:T(8,128)(2,1)} %all-gather.3.cloned.1.call-done, bf16[1,4096,256]{2,1,0:T(8,128)(2,1)S(1)} %copy-done), kind=kOutput, calls=%fused_computation.17 | convolution fusion | flops 1610809344 | bytes 9175040 | tf_op jit(solution)/shard_map/dot_general | solution.py:114
  182.7 2.6 fusion.20
  189.1 2.0 fusion.4
  193.6 2.7 convolution_convert_fusion
  196.3 4.0 %copy.73 = bf16[4,256,1024]{2,1,0:T(8,128)(2,1)} copy(bf16[4,256,1024]{1,2,0:T(8,128)(2,1)} %bitcast.12) | data formatting | bytes 4194304 | tf_op jit(solution)/shard_map/all_to_all | solution.py:120
  200.3 13.5 %all-gather.5.cloned.1.call-done = bf16[768,1024]{1,0:T(8,128)(2,1)} async-done(((bf16[768,256]{1,0:T(8,128)(2,1)}), bf16[768,1024]{1,0:T(8,128)(2,1)}) %all-gather.5.cloned.1.call-update) | async-done | bytes 1572880 | tf_op jit(solution)/shard_map/all_gather | solution.py:122
  213.8 5.0 %convolution_convert_fusion.1 = bf16[768,1024]{1,0:T(8,128)(2,1)} fusion(bf16[768,1024]{1,0:T(8,128)(2,1)} %all-gather.5.cloned.1.call-done, bf16[1024,1024]{1,0:T(8,128)(2,1)} %bitcast.67), kind=kOutput, calls=%fused_computation.15 | convolution fusion | flops 1611399168 | bytes 5242880 | tf_op jit(solution)/shard_map/dot_general | solution.py:121
  218.8 3.6 %reshape.226 = bf16[64,12,1024]{2,1,0:T(8,128)(2,1)} reshape(bf16[768,1024]{1,0:T(8,128)(2,1)} %convolution_convert_fusion.1) | data formatting | bytes 3145728 | tf_op jit(solution)/shard_map/reshape | solution.py:127
  222.4 10.9 %all-to-all-start.2 = ((bf16[64,12,1024]{2,1,0:T(8,128)(2,1)}), bf16[64,12,1024]{2,1,0:T(8,128)(2,1)}, u32[]{:S(2)}, u32[]{:S(2)}) async-start(bf16[64,12,1024]{2,1,0:T(8,128)(2,1)} %reshape.226), calls=%async_computation.3 | async-start | bytes 4194304 | tf_op jit(solution)/shard_map/all_to_all | solution.py:126
  233.7 50.7 %all-to-all-done.2 = bf16[64,12,1024]{2,1,0:T(8,128)(2,1)} async-done(((bf16[64,12,1024]{2,1,0:T(8,128)(2,1)}), bf16[64,12,1024]{2,1,0:T(8,128)(2,1)}, u32[]{:S(2)}, u32[]{:S(2)}) %all-to-all-start.2) | async-done | bytes 1572896 | tf_op jit(solution)/shard_map/all_to_all | solution.py:126
  284.4 3.6 %reshape.227 = bf16[768,1024]{1,0:T(8,128)(2,1)} reshape(bf16[64,12,1024]{2,1,0:T(8,128)(2,1)} %all-to-all-done.2) | data formatting | bytes 3145728 | tf_op jit(solution)/shard_map/reshape | solution.py:133
  288.0 4.3 %gather_fusion.1 = bf16[512,1024]{1,0:T(8,128)(2,1)S(1)} fusion(bf16[768,1024]{1,0:T(8,128)(2,1)} %reshape.227, s32[1024]{0:T(1024)S(1)} %pad_clamp_fusion), kind=kCustom, calls=%fused_computation.1 | custom fusion | bytes 2099200 | tf_op jit(solution)/shard_map/jit(_take)/gather | solution.py:133
  293.6 3.6 %multiply_reduce_fusion = bf16[128,1024]{1,0:T(8,128)(2,1)} fusion(f32[128,4]{1,0:T(8,128)S(1)} %copy.74, bf16[128,4,1024]{2,1,0:T(4,128)(2,1)} %gather.15, pred[128,4]{1,0:T(8,128)(4,1)S(1)} %copy.70), kind=kLoop, calls=%fused_computation.9 | loop fusion | flops 1966080 | bytes 1313280 | tf_op jit(solution)/shard_map/reduce_sum | solution.py:135
  (89 shorter events, 14.9 us)
Async XLA Ops:
  7.2 170.3 %copy-start = (bf16[1,4096,256]{2,1,0:T(8,128)(2,1)S(1)}, bf16[1,4096,256]{2,1,0:T(8,128)(2,1)}, u32[]{:S(2)}) copy-start(bf16[1,4096,256]{2,1,0:T(8,128)(2,1)} %param.21) | copy-start | bytes 6291460
  7.2 3.0 copy-start.1
  7.2 170.3 %all-gather.3.cloned.1.call-start = ((), (), s32[]{:S(2)}) async-start(), calls=%async_computation.5 | async-start | bytes 7864320 | tf_op jit(solution)/shard_map/all_gather | solution.py:113
  7.2 3.2 %copy-start.7 = (s32[128,4]{0,1:T(4,128)S(1)}, s32[128,4]{0,1:T(4,128)}, u32[]{:S(2)}) copy-start(s32[128,4]{0,1:T(4,128)} %param.19) | copy-start | bytes 6148
  97.1 4.6 %copy-start.4 = (bf16[256,128]{1,0:T(8,128)(2,1)S(1)}, bf16[256,128]{1,0:T(8,128)(2,1)}, u32[]{:S(2)}) copy-start(bf16[256,128]{1,0:T(8,128)(2,1)} %param.13) | copy-start | bytes 196612
  97.1 6.6 %copy-start.5 = (bf16[256,128]{1,0:T(8,128)(2,1)S(1)}, bf16[256,128]{1,0:T(8,128)(2,1)}, u32[]{:S(2)}) copy-start(bf16[256,128]{1,0:T(8,128)(2,1)} %param.14) | copy-start | bytes 196612
  97.1 99.2 %all-to-all-start.1 = ((bf16[256,4,1024]{0,2,1:T(8,128)(2,1)}), bf16[256,4,1024]{0,2,1:T(8,128)(2,1)}, u32[]{:S(2)}, u32[]{:S(2)}) async-start(bf16[256,4,1024]{0,2,1:T(8,128)(2,1)} %bitcast.66), calls=%async_computation.2 | async-start | bytes 4194304 | tf_op jit(solution)/shard_map/all_to_all | solution.py:120
  101.7 112.1 %all-gather.5.cloned.1.call-start = ((), (), s32[]{:S(2)}) async-start(), calls=%async_computation.6 | async-start | bytes 1966080 | tf_op jit(solution)/shard_map/all_gather | solution.py:122
  101.8 84.9 %collective-permute-start.1 = (bf16[128,128]{1,0:T(8,128)(2,1)S(1)}, bf16[128,128]{1,0:T(8,128)(2,1)S(1)}, u32[]{:S(2)}, u32[]{:S(2)}) collective-permute-start(bf16[128,128]{1,0:T(8,128)(2,1)S(1)} %slice.20), channel_id=1, source_target_pairs={{0,4},{4,8},{8,12},{12,16},{16,20},{20,24},{24,28},{28,32},{32,36}... | collective-permute-start | bytes 98312 | tf_op jit(solution)/shard_map/ppermute | solution.py:18
  103.7 85.1 %collective-permute-start = (bf16[128,128]{1,0:T(8,128)(2,1)S(1)}, bf16[128,128]{1,0:T(8,128)(2,1)S(1)}, u32[]{:S(2)}, u32[]{:S(2)}) collective-permute-start(bf16[128,128]{1,0:T(8,128)(2,1)S(1)} %slice.18), channel_id=1, source_target_pairs={{0,4},{4,8},{8,12},{12,16},{16,20},{20,24},{24,28},{28,32},{32,36}... | collective-permute-start | bytes 98312 | tf_op jit(solution)/shard_map/ppermute | solution.py:18
  177.5 4.7 %copy-start.9 = (bf16[768,4096]{1,0:T(8,128)(2,1)S(1)}, bf16[768,4096]{1,0:T(8,128)(2,1)}, u32[]{:S(2)}) copy-start(bf16[768,4096]{1,0:T(8,128)(2,1)} %all-gather.3.cloned.1.call-done) | copy-start | bytes 18874372
  177.5 5.2 %copy-start.10 = (bf16[1,4096,256]{2,1,0:T(8,128)(2,1)S(1)}, bf16[1,4096,256]{2,1,0:T(8,128)(2,1)}, u32[]{:S(2)}) copy-start(bf16[1,4096,256]{2,1,0:T(8,128)(2,1)} %param.22) | copy-start | bytes 6291460
  182.7 3.4 %copy-start.6 = (bf16[256,512]{1,0:T(8,128)(2,1)S(1)}, bf16[256,512]{1,0:T(8,128)(2,1)}, u32[]{:S(2)}) copy-start(bf16[256,512]{1,0:T(8,128)(2,1)} %param.12) | copy-start | bytes 786436
  182.7 3.8 %copy-start.11 = (f32[8]{0:T(128)S(1)}, f32[8]{0:T(128)}, u32[]{:S(2)}) copy-start(f32[8]{0:T(128)} %param.15) | copy-start | bytes 100
  185.3 111.9 %reduce-scatter.2.cloned.1.call-start = ((), (), s32[]{:S(2)}) async-start(), calls=%async_computation.4 | async-start | bytes 2621440 | tf_op jit(solution)/shard_map/reduce_scatter | solution.py:83
  189.1 2.2 copy-start.3
  191.3 2.3 copy-start.2
  222.4 11.2 %copy-start.8 = (f32[128,4]{0,1:T(4,128)S(1)}, f32[128,4]{0,1:T(4,128)}, u32[]{:S(2)}) copy-start(f32[128,4]{0,1:T(4,128)} %param.20) | copy-start | bytes 6148
  222.4 62.0 %all-to-all-start.2 = ((bf16[64,12,1024]{2,1,0:T(8,128)(2,1)}), bf16[64,12,1024]{2,1,0:T(8,128)(2,1)}, u32[]{:S(2)}, u32[]{:S(2)}) async-start(bf16[64,12,1024]{2,1,0:T(8,128)(2,1)} %reshape.226), calls=%async_computation.3 | async-start | bytes 4194304 | tf_op jit(solution)/shard_map/all_to_all | solution.py:126
Sparse Core Ops, SparseCore 0:
  93.2 84.2 all-gather.2
  185.5 28.2 all-gather.4
  216.9 33.2 reduce-scatter.1
where the time goes:
time: 305 us; the launch traced here: 304 us
  waiting for transfers between devices  134 us (44%)
  blocking collectives  63.2 us (21%)
  local copies, waits for them, and re-layouts  39.7 us (13%)
  starting transfers between devices  21.2 us (7%)
  matrix products  17.4 us (6%)
  between operations  14.2 us (5%)
  other arithmetic  13.9 us (5%)
    all_gather x1, waiting for transfers between devices, shards(): portion = lax.all_gather(arrived, 'tp', axis=1, tiled=True)  70.1 us
    all_to_all x1, blocking collectives, shards(): lax.all_to_all(outgoing, 'ep', split_axis=0, concat_axis=0, tiled=True)  63.2 us
    all_to_all x1, waiting for transfers between devices, shards(): lax.all_to_all(expert_result.reshape(experts, capacity, col_share), 'ep',...  50.7 us
    all_gather x1, waiting for transfers between devices, shards(): lax.all_gather(activated, 'tp', axis=1, tiled=True)  13.5 us
    all_to_all x1, starting transfers between devices, shards(): lax.all_to_all(expert_result.reshape(experts, capacity, col_share), 'ep',...  10.9 us
    gather x2, local copies, waits for them, and re-layouts, shards(): jnp.take(extended, slot_tok, axis=0).reshape(experts, capacity, col_share)  7.16 us
    unnamed x27, local copies, waits for them, and re-layouts  6.43 us
  transfers between devices with their start and end apart: 7, of which 3 were waited for; matrix products, arithmetic and copies ran while one was open for 15% of the time, Pallas kernels for 0%

commit v1 on v0

--- a/solution.py
+++ b/solution.py
@@ -110,7 +110,22 @@
     arrived = lax.all_to_all(outgoing, "ep", split_axis=0, concat_axis=0, tiled=True).reshape(
         experts * capacity, col_share
     )
-    portion = lax.all_gather(arrived, "tp", axis=1, tiled=True)
+    size, index, rows = (lax.axis_size("tp"), lax.axis_index("tp"), arrived.shape[1])
+    right = [(i_2, (i_2 + 1) % size) for i_2 in range(size)]
+    left = [(i_2, (i_2 - 1) % size) for i_2 in range(size)]
+    out = jnp.zeros((*arrived.shape[:1], size * rows, *arrived.shape[1 + 1 :]), arrived.dtype)
+    out = lax.dynamic_update_slice_in_dim(out, arrived, index * rows, axis=1)
+    from_left = from_right = arrived
+    half = size // 2
+    for hop in range(1, half + 1):
+        from_left = lax.ppermute(from_left, "tp", right)
+        out = lax.dynamic_update_slice_in_dim(out, from_left, (index - hop) % size * rows, axis=1)
+        if hop < size - half:
+            from_right = lax.ppermute(from_right, "tp", left)
+            out = lax.dynamic_update_slice_in_dim(
+                out, from_right, (index + hop) % size * rows, axis=1
+            )
+    portion = out
     gate_pre = jnp.dot(portion, gate_one, preferred_element_type=jnp.float32)
     up_pre = jnp.dot(portion, up_one, preferred_element_type=jnp.float32)
     gate_cut = jnp.minimum(gate_pre, CLAMP)

time: 305 us -> 294 us (0.964)
  waiting for transfers between devices: 134 us -> 117 us
  local copies, waits for them, and re-layouts: 39.7 us -> 45.8 us
    all_gather x1 -> x0, waiting for transfers between devices: 70.1 us -> none  [shards(): portion = lax.all_gather(arrived, 'tp', axis=1, tiled=True)]
    ppermute x0 -> x3, waiting for transfers between devices: none -> 52 us  [the longest x2 52 us: shards(): from_left = lax.ppermute(from_left, 'tp', right)]
    dynamic_update_slice x0 -> x4, local copies, waits for them, and re-layouts: none -> 5.02 us  [the longest x2 3.21 us: shards(): lax.dynamic_update_slice_in_dim(out, from_left, (index - hop) % size * ro...]
    all_to_all x1, waiting for transfers between devices: 0.01 us -> 3.58 us  [shards(): lax.all_to_all(down_weight[0], 'tp', split_axis=1, concat_axis=0, tiled=T...]
    ppermute x0 -> x3, starting transfers between devices: none -> 3.54 us  [the longest x2 1.88 us: shards(): from_left = lax.ppermute(from_left, 'tp', right)]
  transfers between devices with their start and end apart: 7 -> 9, of which waited for: 3 -> 5; matrix products, arithmetic and copies ran while one was open for 15% -> 17% of each run, Pallas kernels for 0% -> 0%
where the time goes in v1:
time: 294 us; the launch traced here: 293 us
  waiting for transfers between devices  117 us (40%)
  blocking collectives  63.2 us (21%)
  local copies, waits for them, and re-layouts  45.8 us (16%)
  starting transfers between devices  23.2 us (8%)
  between operations  14.6 us (5%)
  matrix products  14.5 us (5%)
  other arithmetic  13.9 us (5%)
    all_to_all x1, blocking collectives, shards(): lax.all_to_all(outgoing, 'ep', split_axis=0, concat_axis=0, tiled=True)  63.2 us
    ppermute x2, waiting for transfers between devices, shards(): from_left = lax.ppermute(from_left, 'tp', right)  52 us
    all_to_all x1, waiting for transfers between devices, shards(): lax.all_to_all(expert_result.reshape(experts, capacity, col_share), 'ep',...  50.7 us
    all_gather x1, waiting for transfers between devices, shards(): lax.all_gather(activated, 'tp', axis=1, tiled=True)  11 us
    all_to_all x1, starting transfers between devices, shards(): lax.all_to_all(expert_result.reshape(experts, capacity, col_share), 'ep',...  9.31 us
    gather x2, local copies, waits for them, and re-layouts, shards(): jnp.take(extended, slot_tok, axis=0).reshape(experts, capacity, col_share)  7.16 us
    unnamed x27, local copies, waits for them, and re-layouts  6.72 us
  transfers between devices with their start and end apart: 9, of which 5 were waited for; matrix products, arithmetic and copies ran while one was open for 17% of the time, Pallas kernels for 0%

profile of v1, /device:TPU:2, one launch (start us, length us, event | category | flops | bytes accessed | tf_op | source)
XLA Modules:
  0.0 292.5 jit_solution(1548604688542839236)
XLA Ops:
  7.2 2.9 %convert_element_type.41 = f32[128,4096]{1,0:T(8,128)} convert(bf16[128,4096]{1,0:T(8,128)(2,1)} %param.17) | non-fusion elementwise | flops 524288 | bytes 3145728 | tf_op jit(solution)/shard_map/convert_element_type | solution.py:93
  12.6 2.4 scatter_custom_fusion
  17.0 3.6 %gather_fusion = bf16[768,1024]{1,0:T(8,128)(2,1)} fusion(bf16[129,1024]{1,0:T(8,128)(2,1)S(1)} %concatenate.19, s32[1024]{0:T(1024)S(1)} %pad_clamp_fusion.1), kind=kCustom, calls=%fused_computation | custom fusion | bytes 3148800 | tf_op jit(solution)/shard_map/jit(_take)/gather | solution.py:109
  20.6 3.6 %gather.13 = bf16[64,12,1024]{2,1,0:T(8,128)(2,1)} reshape(bf16[768,1024]{1,0:T(8,128)(2,1)} %gather_fusion) | data formatting | bytes 3145728 | tf_op jit(solution)/shard_map/jit(_take)/gather | solution.py:109
  26.2 63.2 %all_to_all.29 = bf16[64,12,1024]{2,1,0:T(8,128)(2,1)} all-to-all(bf16[64,12,1024]{2,1,0:T(8,128)(2,1)S(1)} %broadcast_select_fusion), channel_id=1, replica_groups=mesh['ep'=64,'tp'=4] {'ep'}, dimensions={0} | all-to-all | bytes 3145728 | tf_op jit(solution)/shard_map/all_to_all | solution.py:110
  89.3 3.6 %reshape.225 = bf16[768,1024]{1,0:T(8,128)(2,1)} reshape(bf16[64,12,1024]{2,1,0:T(8,128)(2,1)} %all_to_all.29) | data formatting | bytes 3145728 | tf_op jit(solution)/shard_map/reshape | solution.py:110
  96.2 33.0 %collective-permute-done.2 = bf16[768,1024]{1,0:T(8,128)(2,1)} collective-permute-done((bf16[768,1024]{1,0:T(8,128)(2,1)}, bf16[768,1024]{1,0:T(8,128)(2,1)}, u32[]{:S(2)}, u32[]{:S(2)}) %collective-permute-start.2) | collective-permute-done | bytes 1572896 | tf_op jit(solution)/shard_map/ppermute | solution.py:121
  129.5 4.1 %copy.72 = bf16[1,256,4096]{1,2,0:T(8,128)(2,1)} copy(bf16[1,256,4096]{2,1,0:T(8,128)(2,1)} %param.23) | data formatting | bytes 4194304 | tf_op args[11]
  133.6 4.6 %all-to-all-start.1 = ((bf16[256,4,1024]{0,2,1:T(8,128)(2,1)}), bf16[256,4,1024]{0,2,1:T(8,128)(2,1)}, u32[]{:S(2)}, u32[]{:S(2)}) async-start(bf16[256,4,1024]{0,2,1:T(8,128)(2,1)} %bitcast.66), calls=%async_computation.2 | async-start | bytes 4194304 | tf_op jit(solution)/shard_map/all_to_all | solution.py:135
  140.2 3.6 %collective-permute-start = (bf16[128,128]{1,0:T(8,128)(2,1)S(1)}, bf16[128,128]{1,0:T(8,128)(2,1)S(1)}, u32[]{:S(2)}, u32[]{:S(2)}) collective-permute-start(bf16[128,128]{1,0:T(8,128)(2,1)S(1)} %slice.18), channel_id=1, source_target_pairs={{0,4},{4,8},{8,12},{12,16},{16,20},{20,24},{24,28},{28,32},{32,36}... | collective-permute-start | bytes 98312 | tf_op jit(solution)/shard_map/ppermute | solution.py:18
  148.9 19.1 %collective-permute-done.4 = bf16[768,1024]{1,0:T(8,128)(2,1)} collective-permute-done((bf16[768,1024]{1,0:T(8,128)(2,1)}, bf16[768,1024]{1,0:T(8,128)(2,1)}, u32[]{:S(2)}, u32[]{:S(2)}) %collective-permute-start.4) | collective-permute-done | bytes 1572896 | tf_op jit(solution)/shard_map/ppermute | solution.py:121
  171.4 2.6 fusion.20
  177.8 2.0 fusion.4
  182.5 2.7 convolution_convert_fusion
  185.2 3.6 %all-to-all-done.1 = bf16[256,4,1024]{0,2,1:T(8,128)(2,1)} async-done(((bf16[256,4,1024]{0,2,1:T(8,128)(2,1)}), bf16[256,4,1024]{0,2,1:T(8,128)(2,1)}, u32[]{:S(2)}, u32[]{:S(2)}) %all-to-all-start.1) | async-done | bytes 2097184 | tf_op jit(solution)/shard_map/all_to_all | solution.py:135
  188.7 4.0 %copy.73 = bf16[4,256,1024]{2,1,0:T(8,128)(2,1)} copy(bf16[4,256,1024]{1,2,0:T(8,128)(2,1)} %bitcast.12) | data formatting | bytes 4194304 | tf_op jit(solution)/shard_map/all_to_all | solution.py:135
  192.7 11.0 %all-gather.2.cloned.1.call-done = bf16[768,1024]{1,0:T(8,128)(2,1)} async-done(((bf16[768,256]{1,0:T(8,128)(2,1)}), bf16[768,1024]{1,0:T(8,128)(2,1)}) %all-gather.2.cloned.1.call-update) | async-done | bytes 1572880 | tf_op jit(solution)/shard_map/all_gather | solution.py:137
  203.8 5.0 %convolution_convert_fusion.1 = bf16[768,1024]{1,0:T(8,128)(2,1)} fusion(bf16[768,1024]{1,0:T(8,128)(2,1)} %all-gather.2.cloned.1.call-done, bf16[1024,1024]{1,0:T(8,128)(2,1)} %bitcast.67), kind=kOutput, calls=%fused_computation.15 | convolution fusion | flops 1611399168 | bytes 5242880 | tf_op jit(solution)/shard_map/dot_general | solution.py:136
  208.8 3.6 %reshape.226 = bf16[64,12,1024]{2,1,0:T(8,128)(2,1)} reshape(bf16[768,1024]{1,0:T(8,128)(2,1)} %convolution_convert_fusion.1) | data formatting | bytes 3145728 | tf_op jit(solution)/shard_map/reshape | solution.py:142
  212.4 9.3 %all-to-all-start.2 = ((bf16[64,12,1024]{2,1,0:T(8,128)(2,1)}), bf16[64,12,1024]{2,1,0:T(8,128)(2,1)}, u32[]{:S(2)}, u32[]{:S(2)}) async-start(bf16[64,12,1024]{2,1,0:T(8,128)(2,1)} %reshape.226), calls=%async_computation.3 | async-start | bytes 4194304 | tf_op jit(solution)/shard_map/all_to_all | solution.py:141
  222.2 50.7 %all-to-all-done.2 = bf16[64,12,1024]{2,1,0:T(8,128)(2,1)} async-done(((bf16[64,12,1024]{2,1,0:T(8,128)(2,1)}), bf16[64,12,1024]{2,1,0:T(8,128)(2,1)}, u32[]{:S(2)}, u32[]{:S(2)}) %all-to-all-start.2) | async-done | bytes 1572896 | tf_op jit(solution)/shard_map/all_to_all | solution.py:141
  272.9 3.6 %reshape.227 = bf16[768,1024]{1,0:T(8,128)(2,1)} reshape(bf16[64,12,1024]{2,1,0:T(8,128)(2,1)} %all-to-all-done.2) | data formatting | bytes 3145728 | tf_op jit(solution)/shard_map/reshape | solution.py:148
  276.5 4.3 %gather_fusion.1 = bf16[512,1024]{1,0:T(8,128)(2,1)S(1)} fusion(bf16[768,1024]{1,0:T(8,128)(2,1)} %reshape.227, s32[1024]{0:T(1024)S(1)} %pad_clamp_fusion), kind=kCustom, calls=%fused_computation.1 | custom fusion | bytes 2099200 | tf_op jit(solution)/shard_map/jit(_take)/gather | solution.py:148
  282.1 3.6 %multiply_reduce_fusion = bf16[128,1024]{1,0:T(8,128)(2,1)} fusion(f32[128,4]{1,0:T(8,128)S(1)} %copy.74, bf16[128,4,1024]{2,1,0:T(4,128)(2,1)} %gather.15, pred[128,4]{1,0:T(8,128)(4,1)S(1)} %copy.70), kind=kLoop, calls=%fused_computation.9 | loop fusion | flops 1966080 | bytes 1313280 | tf_op jit(solution)/shard_map/reduce_sum | solution.py:150
  (97 shorter events, 28.2 us)
Async XLA Ops:
  7.2 162.4 %copy-start = (bf16[1,4096,256]{2,1,0:T(8,128)(2,1)S(1)}, bf16[1,4096,256]{2,1,0:T(8,128)(2,1)}, u32[]{:S(2)}) copy-start(bf16[1,4096,256]{2,1,0:T(8,128)(2,1)} %param.21) | copy-start | bytes 6291460
  7.2 3.0 %copy-start.2 = (bf16[128,4096]{1,0:T(8,128)(2,1)S(1)}, bf16[128,4096]{1,0:T(8,128)(2,1)}, u32[]{:S(2)}) copy-start(bf16[128,4096]{1,0:T(8,128)(2,1)} %param.17) | copy-start | bytes 3145732
  7.2 3.2 %copy-start.8 = (s32[128,4]{0,1:T(4,128)S(1)}, s32[128,4]{0,1:T(4,128)}, u32[]{:S(2)}) copy-start(s32[128,4]{0,1:T(4,128)} %param.19) | copy-start | bytes 6148
  93.0 36.2 %collective-permute-start.2 = (bf16[768,1024]{1,0:T(8,128)(2,1)}, bf16[768,1024]{1,0:T(8,128)(2,1)}, u32[]{:S(2)}, u32[]{:S(2)}) collective-permute-start(bf16[768,1024]{1,0:T(8,128)(2,1)} %reshape.225), channel_id=1, source_target_pairs={{0,1},{1,2},{2,3},{3,0},{4,5},{5,6},{6,7},{7,4},{8,9},{9,10},{10,1... | collective-permute-start | bytes 4718600 | tf_op jit(solution)/shard_map/ppermute | solution.py:121
  94.5 52.7 %collective-permute-start.3 = (bf16[768,1024]{1,0:T(8,128)(2,1)}, bf16[768,1024]{1,0:T(8,128)(2,1)}, u32[]{:S(2)}, u32[]{:S(2)}) collective-permute-start(bf16[768,1024]{1,0:T(8,128)(2,1)} %reshape.225), channel_id=1, source_target_pairs={{0,3},{1,0},{2,1},{3,2},{4,7},{5,4},{6,5},{7,6},{8,11},{9,8},{10,9... | collective-permute-start | bytes 4718600 | tf_op jit(solution)/shard_map/ppermute | solution.py:124
  129.2 38.8 %collective-permute-start.4 = (bf16[768,1024]{1,0:T(8,128)(2,1)}, bf16[768,1024]{1,0:T(8,128)(2,1)}, u32[]{:S(2)}, u32[]{:S(2)}) collective-permute-start(bf16[768,1024]{1,0:T(8,128)(2,1)} %collective-permute-done.2), channel_id=1, source_target_pairs={{0,1},{1,2},{2,3},{3,0},{4,5},{5,6},{6,7},{7,4},{8,9},{9,10},{10,1... | collective-permute-start | bytes 4718600 | tf_op jit(solution)/shard_map/ppermute | solution.py:121
  133.6 4.6 %copy-start.5 = (bf16[256,128]{1,0:T(8,128)(2,1)S(1)}, bf16[256,128]{1,0:T(8,128)(2,1)}, u32[]{:S(2)}) copy-start(bf16[256,128]{1,0:T(8,128)(2,1)} %param.13) | copy-start | bytes 196612
  133.6 6.6 %copy-start.6 = (bf16[256,128]{1,0:T(8,128)(2,1)S(1)}, bf16[256,128]{1,0:T(8,128)(2,1)}, u32[]{:S(2)}) copy-start(bf16[256,128]{1,0:T(8,128)(2,1)} %param.14) | copy-start | bytes 196612
  133.6 55.2 %all-to-all-start.1 = ((bf16[256,4,1024]{0,2,1:T(8,128)(2,1)}), bf16[256,4,1024]{0,2,1:T(8,128)(2,1)}, u32[]{:S(2)}, u32[]{:S(2)}) async-start(bf16[256,4,1024]{0,2,1:T(8,128)(2,1)} %bitcast.66), calls=%async_computation.2 | async-start | bytes 4194304 | tf_op jit(solution)/shard_map/all_to_all | solution.py:135
  138.1 65.6 %all-gather.2.cloned.1.call-start = ((), (), s32[]{:S(2)}) async-start(), calls=%async_computation.5 | async-start | bytes 1966080 | tf_op jit(solution)/shard_map/all_gather | solution.py:137
  138.2 37.2 %collective-permute-start.1 = (bf16[128,128]{1,0:T(8,128)(2,1)S(1)}, bf16[128,128]{1,0:T(8,128)(2,1)S(1)}, u32[]{:S(2)}, u32[]{:S(2)}) collective-permute-start(bf16[128,128]{1,0:T(8,128)(2,1)S(1)} %slice.20), channel_id=1, source_target_pairs={{0,4},{4,8},{8,12},{12,16},{16,20},{20,24},{24,28},{28,32},{32,36}... | collective-permute-start | bytes 98312 | tf_op jit(solution)/shard_map/ppermute | solution.py:18
  140.2 37.4 %collective-permute-start = (bf16[128,128]{1,0:T(8,128)(2,1)S(1)}, bf16[128,128]{1,0:T(8,128)(2,1)S(1)}, u32[]{:S(2)}, u32[]{:S(2)}) collective-permute-start(bf16[128,128]{1,0:T(8,128)(2,1)S(1)} %slice.18), channel_id=1, source_target_pairs={{0,4},{4,8},{8,12},{12,16},{16,20},{20,24},{24,28},{28,32},{32,36}... | collective-permute-start | bytes 98312 | tf_op jit(solution)/shard_map/ppermute | solution.py:18
  144.0 1.4 copy-start.1
  169.6 1.8 copy-start.10
  171.4 3.4 %copy-start.7 = (bf16[256,512]{1,0:T(8,128)(2,1)S(1)}, bf16[256,512]{1,0:T(8,128)(2,1)}, u32[]{:S(2)}) copy-start(bf16[256,512]{1,0:T(8,128)(2,1)} %param.12) | copy-start | bytes 786436
  171.4 3.8 %copy-start.11 = (f32[8]{0:T(128)S(1)}, f32[8]{0:T(128)}, u32[]{:S(2)}) copy-start(f32[8]{0:T(128)} %param.15) | copy-start | bytes 100
  174.1 111.6 %reduce-scatter.2.cloned.1.call-start = ((), (), s32[]{:S(2)}) async-start(), calls=%async_computation.4 | async-start | bytes 2621440 | tf_op jit(solution)/shard_map/reduce_scatter | solution.py:83
  177.8 2.2 copy-start.4
  180.1 2.4 copy-start.3
  212.4 9.7 %copy-start.9 = (f32[128,4]{0,1:T(4,128)S(1)}, f32[128,4]{0,1:T(4,128)}, u32[]{:S(2)}) copy-start(f32[128,4]{0,1:T(4,128)} %param.20) | copy-start | bytes 6148
  212.4 60.5 %all-to-all-start.2 = ((bf16[64,12,1024]{2,1,0:T(8,128)(2,1)}), bf16[64,12,1024]{2,1,0:T(8,128)(2,1)}, u32[]{:S(2)}, u32[]{:S(2)}) async-start(bf16[64,12,1024]{2,1,0:T(8,128)(2,1)} %reshape.226), calls=%async_computation.3 | async-start | bytes 4194304 | tf_op jit(solution)/shard_map/all_to_all | solution.py:141
Sparse Core Ops, SparseCore 0:
  174.2 29.4 all-gather.1
  206.9 31.6 reduce-scatter.1
